TPU v7x, 32 devices: a whole 2x2x4 slice. The times are simulated.
32 devices in a mesh: sp: 8 (over z, x), tp: 4 (over y, core).
Axes of the slice: x: 2, y: 2, z: 4, core: 2. Of those that a mesh axis runs over, the one named last changes fastest.
Arguments:
- tokens: bfloat16 [1024, 2048], P('sp', 'tp'), may hold values from -6 to 6
- conv_value_weight: bfloat16 [2048, 1024], P('sp', 'tp'), may hold values from -0.125 to 0.125
- conv_gate_weight: bfloat16 [2048, 1024], P('sp', 'tp'), may hold values from -0.125 to 0.125
- conv_kernel: bfloat16 [31, 1024], P(None, 'tp'), may hold values from -16 to 16
- conv_norm_gain: float32 [1024], P('tp'), may hold values from 0.1 to 1.9
- query_weight: bfloat16 [2048, 2048], P('sp', 'tp'), may hold values from -0.125 to 0.125
- key_weight: bfloat16 [2048, 2048], P('sp', 'tp'), may hold values from -0.125 to 0.125
- value_weight: bfloat16 [2048, 2048], P('sp', 'tp'), may hold values from -0.125 to 0.125
- input_gate_weight: bfloat16 [2048, 8], P(None, 'tp'), may hold values from -0.125 to 0.125
- forget_gate_weight: bfloat16 [2048, 8], P(None, 'tp'), may hold values from -0.125 to 0.125
- input_offset: float32 [1024, 8], P('sp', 'tp'), may hold values from -4 to 210
- forget_offset: float32 [1024, 8], P('sp', 'tp'), may hold values from 0 to 30
- memory_norm_gain: float32 [2048], P('tp'), may hold values from 0.1 to 1.9
- conv_out_weight: bfloat16 [1024, 2048], P('tp', 'sp'), may hold values from -0.3125 to 0.3125
- memory_out_weight: bfloat16 [2048, 2048], P('tp', 'sp'), may hold values from -0.125 to 0.125
Outputs:
- mixed: bfloat16 [1024, 2048], P('sp', 'tp')
All inputs are finite; a program needn't handle non-finite values.
Results may differ from a plain program's by a relative error of at most 0.03.
Values may be sent and summed in bfloat16 or wider, within the bound.
A program may use at most 128 MiB of HBM per device.

v0:
```python
import jax
import jax.numpy as jnp
from jax import lax
from jax.sharding import PartitionSpec as P

BLOCK = 64
EPS = 1e-06
LOWEST_LEVEL = -1e30


def shifted_2(value, axis, steps):
    count = lax.axis_size(axis)
    leading, last = (max(0, -steps), min(count, count - steps))
    return lax.ppermute(value, axis, [(source, source + steps) for source in range(leading, last)])


def carried_in(shard, axis, join, neutral):
    place = lax.axis_index(axis)
    gathered = jax.tree.map(
        lambda a, kind: lax.all_gather(a.astype(kind), axis),
        shard,
        (jnp.bfloat16, jnp.bfloat16, jnp.bfloat16, jnp.bfloat16),
    )
    state = jax.tree.map(lambda a, e: jnp.zeros_like(a) + jnp.asarray(e, a.dtype), shard, neutral)

    def one(step, state):
        return join(
            state,
            jax.tree.map(
                lambda a, own: lax.dynamic_index_in_dim(a, step, 0, False).astype(own.dtype),
                gathered,
                shard,
            ),
        )

    return lax.fori_loop(0, place, one, state)


def block_step(carry, inputs):
    state, normal, level = carry
    query, key, value, gate_in, forget_log = inputs
    length = gate_in.shape[-1]
    scale = query.shape[-1] ** (-0.5)
    causal = jnp.tril(jnp.ones((length, length), dtype=bool))
    within = jnp.cumsum(forget_log, axis=-1)
    log_weight = within[:, :, None] - within[:, None, :] + gate_in[:, None, :]
    log_weight = jnp.where(causal, log_weight, -jnp.inf)
    carried = within + level[:, None]
    top = jnp.maximum(carried, jnp.max(log_weight, axis=-1))
    weight = jnp.exp(log_weight - top[:, :, None])
    carried_weight = jnp.exp(carried - top) * scale
    scores = jnp.einsum("htd,hsd->hts", query, key, preferred_element_type=jnp.float32) * (
        scale * weight
    )
    numer = jnp.einsum(
        "hts,hse->hte", scores.astype(jnp.bfloat16), value, preferred_element_type=jnp.float32
    )
    numer = numer + carried_weight[:, :, None] * jnp.einsum(
        "hed,htd->hte", state.astype(jnp.bfloat16), query, preferred_element_type=jnp.float32
    )
    denom = jnp.sum(scores, axis=-1) + carried_weight * jnp.einsum(
        "hd,htd->ht", normal.astype(jnp.bfloat16), query, preferred_element_type=jnp.float32
    )
    result = numer / jnp.maximum(jnp.abs(denom), 1.0)[:, :, None]
    last = within[:, -1]
    end_log = last[:, None] - within + gate_in
    new_level = jnp.maximum(last + level, jnp.max(end_log, axis=-1))
    keep = jnp.exp(last + level - new_level)
    fresh = jnp.exp(end_log - new_level[:, None])
    scaled_key = (fresh[:, :, None] * key).astype(jnp.bfloat16)
    new_state = keep[:, None, None] * state + jnp.einsum(
        "hse,hsd->hed", value, scaled_key, preferred_element_type=jnp.float32
    )
    new_normal = keep[:, None] * normal + jnp.sum(scaled_key.astype(jnp.float32), axis=1)
    return ((new_state, new_normal, new_level), result)


def depthwise(extended, kernel):
    taps = kernel.shape[0]
    length = extended.shape[0] - taps + 1
    total = extended[0:length] * kernel[0]
    for index in range(1, taps):
        total = total + extended[index : index + length] * kernel[index]
    return total


def merge_states(first, second):
    first_state, first_normal, first_level, first_total = first
    second_state, second_normal, second_level, second_total = second
    shifted = first_level + second_total
    level = jnp.maximum(shifted, second_level)
    older = jnp.exp(shifted - level)
    newer = jnp.exp(second_level - level)
    state = older[:, None, None] * first_state + newer[:, None, None] * second_state
    normal = older[:, None] * first_normal + newer[:, None] * second_normal
    return (state, normal, level, first_total + second_total)


def on_device_by_position(
    tokens,
    conv_value_weight,
    conv_gate_weight,
    conv_kernel,
    conv_norm_gain,
    query_weight,
    key_weight,
    value_weight,
    input_gate_weight,
    forget_gate_weight,
    input_offset,
    forget_offset,
    memory_norm_gain,
    conv_out_weight,
    memory_out_weight,
):
    length = tokens.shape[0]
    heads_here = input_gate_weight.shape[1]
    whole = lax.all_gather(tokens, "tp", axis=1, tiled=True)
    pieces = (
        lax.all_gather(conv_value_weight, "sp", axis=0, tiled=True),
        lax.all_gather(conv_gate_weight, "sp", axis=0, tiled=True),
        lax.all_gather(query_weight, "sp", axis=0, tiled=True),
        lax.all_gather(key_weight, "sp", axis=0, tiled=True),
        lax.all_gather(value_weight, "sp", axis=0, tiled=True),
    )
    folded = tuple((jnp.dot(whole, piece, preferred_element_type=jnp.float32) for piece in pieces))
    conv_value, conv_gate, query_flat, key_flat, value_flat = folded
    gate_pre = jnp.dot(whole, input_gate_weight, preferred_element_type=jnp.float32)
    forget_pre = jnp.dot(whole, forget_gate_weight, preferred_element_type=jnp.float32)
    glu = (conv_value * jax.nn.sigmoid(conv_gate)).astype(jnp.bfloat16)
    taps = conv_kernel.shape[0]
    head_dim = query_flat.shape[1] // heads_here

    def to_heads(flat):
        return flat.astype(jnp.bfloat16).reshape(length, heads_here, head_dim).transpose(1, 0, 2)

    query = to_heads(query_flat)
    key = to_heads(key_flat)
    value = to_heads(value_flat)
    gate_in = (gate_pre + input_offset).T
    forget_log = jax.nn.log_sigmoid(forget_pre + forget_offset).T
    within = jnp.cumsum(forget_log, axis=1)
    total = within[:, -1]
    end_log = total[:, None] - within + gate_in
    local_level = jnp.max(end_log, axis=1)
    fresh = jnp.exp(end_log - local_level[:, None])
    scaled_key = (fresh[:, :, None] * key).astype(jnp.bfloat16)
    local_state = jnp.einsum("hse,hsd->hed", value, scaled_key, preferred_element_type=jnp.float32)
    local_normal = jnp.sum(scaled_key.astype(jnp.float32), axis=1)
    blank_state = (
        jnp.zeros_like(local_state),
        jnp.zeros_like(local_normal),
        jnp.full_like(local_level, LOWEST_LEVEL),
        jnp.zeros_like(total),
    )
    prior = shifted_2(glu[length - (taps - 1) :], "sp", 1)
    incoming = carried_in(
        (local_state, local_normal, local_level, total), "sp", merge_states, blank_state
    )
    extended = jnp.concatenate([prior, glu], axis=0).astype(jnp.float32)
    conv = depthwise(extended, conv_kernel.astype(jnp.float32))
    blocks = length // BLOCK

    def split(array):
        return jnp.moveaxis(array.reshape((heads_here, blocks, BLOCK) + array.shape[2:]), 1, 0)

    _, hidden = lax.scan(
        block_step,
        tuple(incoming[:3]),
        (split(query), split(key), split(value), split(gate_in), split(forget_log)),
    )
    hidden = jnp.moveaxis(hidden, 0, 1).reshape(heads_here, length, head_dim)
    hidden_squares = jnp.sum(hidden * hidden, axis=(0, 2))
    channel_sum, channel_squares, memory_squares = lax.psum(
        (jnp.sum(conv, axis=1), jnp.sum(conv * conv, axis=1), hidden_squares), "tp"
    )
    channels = conv.shape[1] * lax.axis_size("tp")
    mean = (channel_sum / channels)[:, None]
    variance = (channel_squares / channels)[:, None] - mean * mean
    conv_branch = jax.nn.silu((conv - mean) * lax.rsqrt(variance + EPS) * conv_norm_gain).astype(
        jnp.bfloat16
    )
    entries = heads_here * head_dim * lax.axis_size("tp")
    memory_scale = lax.rsqrt(memory_squares / entries + EPS)
    hidden = hidden * memory_scale[None, :, None]
    hidden = hidden * memory_norm_gain.reshape(heads_here, 1, head_dim)
    memory_branch = (
        hidden.transpose(1, 0, 2).reshape(length, heads_here * head_dim).astype(jnp.bfloat16)
    )
    conv_columns, memory_columns = (
        lax.all_gather(conv_out_weight, "sp", axis=1, tiled=True),
        lax.all_gather(memory_out_weight, "sp", axis=1, tiled=True),
    )
    contract = (((0,), (1,)), ((), ()))
    summed = lax.psum_scatter(
        (
            lax.dot_general(conv_columns, conv_branch, contract, preferred_element_type=jnp.float32)
            + lax.dot_general(
                memory_columns, memory_branch, contract, preferred_element_type=jnp.float32
            )
        ).astype(jnp.bfloat16),
        "tp",
        scatter_dimension=0,
        tiled=True,
    ).astype(jnp.float32)
    return summed.T.astype(jnp.bfloat16)


def forget_parts(forget_log):
    coarse = jnp.round(forget_log * 8.0) * 0.125
    return (jnp.cumsum(coarse, axis=-1), jnp.cumsum(forget_log - coarse, axis=-1))


def exchange_weights(pieces):
    return lax.all_to_all(pieces, "sp", 0, 0, tiled=False)


def gather_tokens(tokens):
    whole = lax.all_gather(tokens, "tp", axis=1, tiled=True)
    return lax.all_gather(whole, "sp", axis=0, tiled=True)


def gather_in_group(mine, size):
    count = lax.axis_size("sp")
    groups = [list(range(first, first + size)) for first in range(0, count, size)]
    return lax.all_gather(mine, "sp", axis_index_groups=groups)


def on_device_by_column(
    tokens,
    conv_value_weight,
    conv_gate_weight,
    conv_kernel,
    conv_norm_gain,
    query_weight,
    key_weight,
    value_weight,
    input_gate_weight,
    forget_gate_weight,
    input_offset,
    forget_offset,
    memory_norm_gain,
    conv_out_weight,
    memory_out_weight,
):
    f32, bf16 = (jnp.float32, jnp.bfloat16)
    count = lax.axis_size("sp")
    columns = lax.axis_size("tp")
    place = lax.axis_index("sp")
    heads_here = input_gate_weight.shape[1]
    size = count // heads_here
    head, quarter = (place // size, place % size)
    depth = query_weight.shape[0]
    head_dim = query_weight.shape[1] // heads_here
    slab = head_dim // size
    channels = conv_value_weight.shape[1] // count
    pieces = jnp.concatenate(
        [
            w.reshape(depth, count, -1)
            for w in (query_weight, key_weight, value_weight, conv_value_weight, conv_gate_weight)
        ],
        axis=2,
    ).transpose(1, 0, 2)
    weights = exchange_weights(pieces).reshape(count * depth, -1)
    whole = gather_tokens(tokens)
    length = whole.shape[0]
    offsets = lax.all_gather(
        jnp.concatenate([input_offset, forget_offset], axis=1), "sp", axis=0, tiled=True
    )
    gate_weights = jnp.concatenate([input_gate_weight, forget_gate_weight], axis=1)
    flat = jnp.dot(whole, weights, preferred_element_type=f32)
    gates = (jnp.dot(whole, gate_weights, preferred_element_type=f32) + offsets).T
    glu = (
        flat[:, 3 * slab : 3 * slab + channels] * jax.nn.sigmoid(flat[:, 3 * slab + channels :])
    ).astype(bf16)
    parts = gather_in_group(flat[:, : 3 * slab].astype(bf16), size)
    taps = conv_kernel.shape[0]
    kernel = lax.dynamic_slice_in_dim(conv_kernel, place * channels, channels, 1).astype(f32)
    extended = jnp.concatenate([jnp.zeros((taps - 1, channels), f32), glu.astype(f32)], axis=0)
    conv = depthwise(extended, kernel)
    rows = length // size
    start = quarter * rows
    gate_in = lax.dynamic_index_in_dim(gates[:heads_here], head, 0, False)
    forget_log = jax.nn.log_sigmoid(lax.dynamic_index_in_dim(gates[heads_here:], head, 0, False))
    coarse, fine = forget_parts(forget_log)
    mine_coarse = lax.dynamic_slice_in_dim(coarse, start, rows)
    mine_fine = lax.dynamic_slice_in_dim(fine, start, rows)
    log_weight = (
        mine_coarse[:, None]
        - coarse[None, :]
        + (mine_fine[:, None] - fine[None, :])
        + gate_in[None, :]
    )
    causal = (start + jnp.arange(rows))[:, None] >= jnp.arange(length)[None, :]
    log_weight = jnp.where(causal, log_weight, -jnp.inf)
    weight = jnp.exp(log_weight - jnp.max(log_weight, axis=1, keepdims=True))
    query = lax.dynamic_slice_in_dim(parts[:, :, :slab], start, rows, 1)
    query = query.transpose(1, 0, 2).reshape(rows, head_dim)
    key = parts[:, :, slab : 2 * slab].transpose(1, 0, 2).reshape(length, head_dim)
    value = parts[:, :, 2 * slab :].transpose(1, 0, 2).reshape(length, head_dim)
    scores = jnp.einsum("td,sd->ts", query, key, preferred_element_type=f32) * (
        weight * head_dim ** (-0.5)
    )
    numer = jnp.dot(scores.astype(bf16), value, preferred_element_type=f32)
    denom = jnp.sum(scores, axis=1)
    cell = numer / jnp.maximum(jnp.abs(denom), 1.0)[:, None]
    squares = lax.dynamic_update_slice_in_dim(
        jnp.zeros((length,), f32), jnp.sum(cell * cell, axis=1), start, 0
    )
    sums = lax.psum(
        jnp.stack([jnp.sum(conv, axis=1), jnp.sum(conv * conv, axis=1), squares]), ("sp", "tp")
    )
    total = channels * count * columns
    mean = sums[0] / total
    variance = sums[1] / total - mean * mean
    gain = lax.dynamic_slice_in_dim(conv_norm_gain, place * channels, channels)
    conv_branch = jax.nn.silu(
        (conv - mean[:, None]) * lax.rsqrt(variance + EPS)[:, None] * gain
    ).astype(bf16)
    entries = heads_here * head_dim * columns
    memory_scale = lax.rsqrt(lax.dynamic_slice_in_dim(sums[2], start, rows) / entries + EPS)
    memory_gain = lax.dynamic_slice_in_dim(memory_norm_gain, head * head_dim, head_dim)
    memory_branch = (cell * memory_scale[:, None] * memory_gain).astype(bf16)
    conv_all = lax.all_gather(conv_branch, "sp")
    memory_all = lax.all_gather(memory_branch, "sp")
    conv_all = conv_all.transpose(1, 0, 2).reshape(length, -1)
    memory_all = (
        memory_all.reshape(heads_here, length, head_dim).transpose(1, 0, 2).reshape(length, -1)
    )
    partial = (
        jnp.dot(conv_all, conv_out_weight, preferred_element_type=f32)
        + jnp.dot(memory_all, memory_out_weight, preferred_element_type=f32)
    ).astype(bf16)
    return send_partials(partial)


def send_partials(partial):
    count, columns = (lax.axis_size("sp"), lax.axis_size("tp"))
    length, width = partial.shape
    swapped = lax.all_to_all(partial.reshape(count, length // count, width), "sp", 0, 0)
    swapped = swapped.reshape(columns, count // columns, length // count, width)
    groups = lax.all_to_all(swapped, "tp", 0, 0)
    summed = jnp.sum(groups.astype(jnp.float32), axis=0).astype(jnp.bfloat16)
    return summed.transpose(1, 0, 2).reshape(length // count, -1)


def splits_by_column(mesh, tokens, query_weight, conv_value_weight, input_gate_weight):
    count, columns = (mesh.shape["sp"], mesh.shape["tp"])
    heads_here = input_gate_weight.shape[1] // columns
    head_dim = query_weight.shape[1] // input_gate_weight.shape[1]
    if count % heads_here or count % columns:
        return False
    size = count // heads_here
    return (
        tokens.size * 2 <= 8 * 2**20
        and head_dim % size == 0
        and (tokens.shape[0] % (size * 8) == 0)
        and (conv_value_weight.shape[1] % (count * columns) == 0)
    )


def solution(mesh):
    in_specs = (
        P("sp", "tp"),
        P("sp", "tp"),
        P("sp", "tp"),
        P(None, "tp"),
        P("tp"),
        P("sp", "tp"),
        P("sp", "tp"),
        P("sp", "tp"),
        P(None, "tp"),
        P(None, "tp"),
        P("sp", "tp"),
        P("sp", "tp"),
        P("tp"),
        P("tp", "sp"),
        P("tp", "sp"),
    )
    out_specs = P("sp", "tp")

    def run(*arrays):
        by_column = splits_by_column(mesh, arrays[0], arrays[5], arrays[1], arrays[8])
        on_device = on_device_by_column if by_column else on_device_by_position
        return jax.shard_map(
            on_device, mesh=mesh, in_specs=in_specs, out_specs=out_specs, check_vma=False
        )(*arrays)

    return run
```

profile of v0, /device:TPU:0, one launch (start us, length us, event | category | flops | bytes accessed | tf_op | source)
XLA Modules:
  0.0 270.2 jit_solution(7886336359932702150)
XLA Ops:
  6.6 10.4 %all_gather.27 = bf16[128,2048]{1,0:T(8,128)(2,1)} all-gather(bf16[128,512]{1,0:T(8,128)(2,1)} %param.15), channel_id=1, replica_groups=mesh['sp'=8,'tp'=4] {'tp'}, dimensions={1}, use_global_device_ids=true | all-gather | bytes 655360 | tf_op jit(solution)/shard_map/all_gather | solution.py:219
  17.0 1.1 copy.40
  18.1 1.1 copy.41
  19.2 1.1 copy.42
  20.3 1.0 copy.43
  21.3 1.0 copy.44
  22.3 0.7 constant_dynamic-update-slice_fusion.4
  23.0 0.7 constant_dynamic-update-slice_fusion.3
  23.7 0.7 constant_dynamic-update-slice_fusion.2
  24.4 0.7 constant_dynamic-update-slice_fusion.1
  25.1 0.7 constant_dynamic-update-slice_fusion
  25.8 5.8 %all-to-all-start = ((bf16[8,256,256]{1,2,0:T(8,128)(2,1)}), bf16[8,256,256]{1,2,0:T(8,128)(2,1)S(1)}, u32[]{:S(2)}, u32[]{:S(2)}) async-start(bf16[8,256,256]{1,2,0:T(8,128)(2,1)} %bitcast.5), calls=%async_computation | async-start | bytes 2097152 | tf_op jit(solution)/shard_map/all_to_all | solution.py:215
  31.7 0.1 dynamic-slice_convert_fusion
  31.8 37.1 %all-to-all-done = bf16[8,256,256]{1,2,0:T(8,128)(2,1)S(1)} async-done(((bf16[8,256,256]{1,2,0:T(8,128)(2,1)}), bf16[8,256,256]{1,2,0:T(8,128)(2,1)S(1)}, u32[]{:S(2)}, u32[]{:S(2)}) %all-to-all-start) | async-done | bytes 1048608 | tf_op jit(solution)/shard_map/all_to_all | solution.py:215
  68.9 0.5 copy.45
  69.4 37.1 %all-gather.7.cloned.1.call-done = bf16[1024,2048]{1,0:T(8,128)(2,1)} async-done(((bf16[128,2048]{1,0:T(8,128)(2,1)}), bf16[1024,2048]{1,0:T(8,128)(2,1)}) %all-gather.7.cloned.1.call-update) | async-done | bytes 4194320 | tf_op jit(solution)/shard_map/all_gather | solution.py:220
  106.5 3.5 %convolution_bitcast_fusion.1 = f32[1024,256]{0,1:T(8,128)S(1)} fusion(bf16[2048,256]{1,0:T(8,128)(2,1)S(1)} %bitcast.143, bf16[1024,2048]{1,0:T(8,128)(2,1)} %all-gather.7.cloned.1.call-done), kind=kOutput, calls=%fused_computation.3 | convolution fusion | flops 1073741824 | bytes 6291456 | tf_op jit(solution)/shard_map/dot_general | solution.py:271
  110.0 0.8 slice.659
  110.9 0.1 dynamic_slice.36
  111.0 27.4 %all_gather.31 = f32[1024,4]{0,1:T(4,128)S(1)} all-gather(f32[128,4]{0,1:T(4,128)S(1)} %pad_maximum_fusion.1), channel_id=1, replica_groups=mesh['sp'=8,'tp'=4] {'sp'}, dimensions={0}, use_global_device_ids=true | all-gather | bytes 18432 | tf_op jit(solution)/shard_map/all_gather | solution.py:267
  138.5 3.4 %fusion.3 = f32[4,1024]{1,0:T(4,128)S(1)} fusion(f32[1024,4]{0,1:T(4,128)S(1)} %all_gather.31, bf16[1024,2048]{1,0:T(8,128)(2,1)} %all-gather.7.cloned.1.call-done, bf16[2048,2]{0,1:T(2,128)(2,1)S(1)} %copy-done.2, bf16[2048,2]{0,1:T(2,128)(2,1)S(1)} %copy-done.3), kind=kOutput, calls=%fused_computation.8 | convolution fusion | flops 16814080 | bytes 4243456 | tf_op jit(solution)/shard_map/dot_general | solution.py:272
  141.9 0.3 reduce-window.24
  142.2 0.1 slice.300
  142.3 0.3 reduce-window.16
  142.7 0.1 slice_reduce_fusion
  142.8 0.1 slice_reduce_fusion.1
  143.1 0.5 fusion.4
  143.6 1.3 fusion.81
  144.9 0.4 all-gather.9.cloned.1.call-done
  145.3 2.9 %reshape.162 = bf16[4,1024,192]{1,0,2:T(4,128)(2,1)S(1)} reshape(bf16[4096,192]{0,1:T(8,128)(2,1)} %all-gather.9.cloned.1.call-done) | data formatting | bytes 3145728 | tf_op jit(solution)/shard_map/all_gather | solution.py:226
  148.2 0.5 fusion.83
  148.8 0.7 fusion.85
  149.5 0.2 copy.56
  149.7 0.4 multiply_reduce_fusion
  150.1 39.6 %psum.7 = f32[3,1024]{1,0:T(4,128)S(1)} all-reduce(f32[3,1024]{1,0:T(4,128)S(1)} %pad_maximum_fusion), channel_id=1, replica_groups=mesh['sp'=8,'tp'=4] {'sp','tp'}, use_global_device_ids=true, to_apply=%region_9.10 | all-reduce | flops 3072 | bytes 24576 | tf_op jit(solution)/shard_map/psum | solution.py:310
  189.8 0.8 multiply_convert_fusion
  190.6 0.1 dynamic_slice.34
  190.6 0.1 multiply_convert_fusion.1
  190.8 31.8 %all-gather.1 = bf16[8192,32]{0,1:T(8,128)(2,1)S(1)} all-gather(bf16[1024,32]{0,1:T(8,128)(2,1)S(1)} %multiply_convert_fusion.1), channel_id=3, replica_groups=mesh['sp'=8,'tp'=4] {'sp'}, dimensions={0}, use_global_device_ids=true | all-gather | bytes 589824 | tf_op jit(solution)/shard_map/all_gather | solution.py:324
  222.6 9.4 %all-gather.11.cloned.1.call-done = bf16[2048,256]{0,1:T(8,128)(2,1)} async-done(((bf16[256,256]{0,1:T(8,128)(2,1)}), bf16[2048,256]{0,1:T(8,128)(2,1)}) %all-gather.11.cloned.1.call-update) | async-done | bytes 1048592 | tf_op jit(solution)/shard_map/all_gather | solution.py:325
  232.0 1.3 copy.69
  233.3 0.5 fusion.86
  233.8 0.4 fusion.1
  234.2 17.2 %all_to_all.15 = bf16[8,128,256]{2,1,0:T(8,128)(2,1)S(1)} all-to-all(bf16[8,128,256]{2,1,0:T(8,128)(2,1)S(1)} %bitcast.139), channel_id=1, replica_groups=mesh['sp'=8,'tp'=4] {'sp'}, dimensions={0} | all-to-all | bytes 1048576 | tf_op jit(solution)/shard_map/all_to_all | solution.py:340
  251.3 11.3 %all_to_all.16 = bf16[4,2,128,256]{3,2,1,0:T(8,128)(2,1)S(1)} all-to-all(bf16[4,2,128,256]{3,2,1,0:T(8,128)(2,1)S(1)} %bitcast.141), channel_id=1, replica_groups=mesh['sp'=8,'tp'=4] {'tp'}, dimensions={0} | all-to-all | bytes 1048576 | tf_op jit(solution)/shard_map/all_to_all | solution.py:342
  262.7 0.1 reduce_sum.52
  262.8 0.1 copy.51
  262.9 0.8 copy.52
  (48 shorter events, 0.8 us)
Async XLA Ops:
  6.5 226.8 %copy-start = (bf16[512,256]{1,0:T(8,128)(2,1)S(1)}, bf16[512,256]{1,0:T(8,128)(2,1)}, u32[]{:S(2)}) copy-start(bf16[512,256]{1,0:T(8,128)(2,1)} %param.29) | copy-start | bytes 786436
  6.5 25.1 %copy-start.5 = (f32[128,2]{0,1:T(2,128)S(1)}, f32[128,2]{0,1:T(2,128)}, u32[]{:S(2)}) copy-start(f32[128,2]{0,1:T(2,128)} %param.26) | copy-start | bytes 3076
  6.5 25.1 %copy-start.6 = (f32[128,2]{0,1:T(2,128)S(1)}, f32[128,2]{0,1:T(2,128)}, u32[]{:S(2)}) copy-start(f32[128,2]{0,1:T(2,128)} %param.25) | copy-start | bytes 3076
  6.5 25.1 %copy-start.4 = (bf16[31,256]{1,0:T(8,128)(2,1)S(1)}, bf16[31,256]{1,0:T(8,128)(2,1)}, u32[]{:S(2)}) copy-start(bf16[31,256]{1,0:T(8,128)(2,1)} %param.18) | copy-start | bytes 47620
  6.5 99.9 %all-gather.7.cloned.1.call-start = ((), (), s32[]{:S(2)}) async-start(), calls=%async_computation.3 | async-start | bytes 4718592 | tf_op jit(solution)/shard_map/all_gather | solution.py:220
  25.8 43.1 %all-to-all-start = ((bf16[8,256,256]{1,2,0:T(8,128)(2,1)}), bf16[8,256,256]{1,2,0:T(8,128)(2,1)S(1)}, u32[]{:S(2)}, u32[]{:S(2)}) async-start(bf16[8,256,256]{1,2,0:T(8,128)(2,1)} %bitcast.5), calls=%async_computation | async-start | bytes 2097152 | tf_op jit(solution)/shard_map/all_to_all | solution.py:215
  31.6 113.7 %all-gather.9.cloned.1.call-start = ((), (), s32[]{:S(2)}) async-start(), calls=%async_computation.4 | async-start | bytes 1966080 | tf_op jit(solution)/shard_map/all_gather | solution.py:226
  106.5 4.5 %copy-start.7 = (f32[512]{0:T(512)S(1)}, f32[512]{0:T(512)}, u32[]{:S(2)}) copy-start(f32[512]{0:T(512)} %param.27) | copy-start | bytes 6148
  106.5 32.0 %copy-start.2 = (bf16[2048,2]{0,1:T(2,128)(2,1)S(1)}, bf16[2048,2]{0,1:T(2,128)(2,1)}, u32[]{:S(2)}) copy-start(bf16[2048,2]{0,1:T(2,128)(2,1)} %param.24) | copy-start | bytes 24580
  106.5 32.0 %copy-start.3 = (bf16[2048,2]{0,1:T(2,128)(2,1)S(1)}, bf16[2048,2]{0,1:T(2,128)(2,1)}, u32[]{:S(2)}) copy-start(bf16[2048,2]{0,1:T(2,128)(2,1)} %param.23) | copy-start | bytes 24580
  110.8 121.2 %all-gather.11.cloned.1.call-start = ((), (), s32[]{:S(2)}) async-start(), calls=%async_computation.5 | async-start | bytes 1179648 | tf_op jit(solution)/shard_map/all_gather | solution.py:325
  148.8 41.8 %copy-start.8 = (f32[256]{0:T(256)S(1)}, f32[256]{0:T(256)}, u32[]{:S(2)}) copy-start(f32[256]{0:T(256)} %param.19) | copy-start | bytes 3076
  149.7 84.1 %copy-start.1 = (bf16[256,256]{1,0:T(8,128)(2,1)S(1)}, bf16[256,256]{1,0:T(8,128)(2,1)}, u32[]{:S(2)}) copy-start(bf16[256,256]{1,0:T(8,128)(2,1)} %param.28) | copy-start | bytes 393220
Sparse Core Ops, SparseCore 0:
  17.1 89.3 all-gather.6
  110.9 34.2 all-gather.8
  190.7 41.2 all-gather.10
where the time goes:
time: 271 us; the launch traced here: 270 us
  blocking collectives  138 us (51%)
  waiting for transfers between devices  83.9 us (31%)
  local copies, waits for them, and re-layouts  16.7 us (6%)
  between operations  13.5 us (5%)
  matrix products  8.81 us (3%)
  starting transfers between devices  5.92 us (2%)
  other arithmetic  3.6 us (1%)
    psum x1, blocking collectives, on_device_by_column(): lax.psum(jnp.stack([jnp.sum(conv, axis=1), jnp.sum(conv * conv, axis=1),...  39.6 us
    all_to_all x1, waiting for transfers between devices, exchange_weights(): return lax.all_to_all(pieces, 'sp', 0, 0, tiled=False)  37.1 us
    all_gather x1, waiting for transfers between devices, gather_tokens(): return lax.all_gather(whole, 'sp', axis=0, tiled=True)  37.1 us
    all_gather x1, blocking collectives, on_device_by_column(): conv_all = lax.all_gather(conv_branch, 'sp')  31.8 us
    all_gather x1, blocking collectives, on_device_by_column(): lax.all_gather(jnp.concatenate([input_offset, forget_offset], axis=1), 's...  27.4 us
    all_to_all x1, blocking collectives, send_partials(): lax.all_to_all(partial.reshape(count, length // count, width), 'sp', 0, 0)  17.2 us
    all_to_all x1, blocking collectives, send_partials(): groups = lax.all_to_all(swapped, 'tp', 0, 0)  11.3 us
    all_gather x1, blocking collectives, gather_tokens(): whole = lax.all_gather(tokens, 'tp', axis=1, tiled=True)  10.4 us
  transfers between devices with their start and end apart: 4, of which 4 were waited for; matrix products, arithmetic and copies ran while one was open for 6% of the time, Pallas kernels for 0%

commit v1 on v0

--- a/solution.py
+++ b/solution.py
@@ -307,9 +307,9 @@
     squares = lax.dynamic_update_slice_in_dim(
         jnp.zeros((length,), f32), jnp.sum(cell * cell, axis=1), start, 0
     )
-    sums = lax.psum(
-        jnp.stack([jnp.sum(conv, axis=1), jnp.sum(conv * conv, axis=1), squares]), ("sp", "tp")
-    )
+    block = jnp.stack([jnp.sum(conv, axis=1), jnp.sum(conv * conv, axis=1), squares])
+    shards = lax.all_gather(block, ("sp", "tp"))
+    sums = jnp.sum(shards, axis=0)
     total = channels * count * columns
     mean = sums[0] / total
     variance = sums[1] / total - mean * mean

time: 271 us -> 269 us (level)
  waiting for transfers between devices: 83.9 us -> 79.3 us
    all_gather x0 -> x1, blocking collectives: none -> 41.8 us  [on_device_by_column(): shards = lax.all_gather(block, ('sp', 'tp'))]
    psum x1 -> x0, blocking collectives: 39.6 us -> none  [on_device_by_column(): lax.psum(jnp.stack([jnp.sum(conv, axis=1), jnp.sum(conv * conv, axis=1),...]
    all_gather x1, waiting for transfers between devices: 9.39 us -> 4.7 us  [on_device_by_column(): memory_all = lax.all_gather(memory_branch, 'sp')]
where the time goes in v1:
time: 269 us; the launch traced here: 268 us
  blocking collectives  140 us (52%)
  waiting for transfers between devices  79.3 us (29%)
  local copies, waits for them, and re-layouts  16.7 us (6%)
  between operations  13.5 us (5%)
  matrix products  8.82 us (3%)
  starting transfers between devices  5.92 us (2%)
  other arithmetic  3.7 us (1%)
    all_gather x1, blocking collectives, on_device_by_column(): shards = lax.all_gather(block, ('sp', 'tp'))  41.8 us
    all_to_all x1, waiting for transfers between devices, exchange_weights(): return lax.all_to_all(pieces, 'sp', 0, 0, tiled=False)  37.1 us
    all_gather x1, waiting for transfers between devices, gather_tokens(): return lax.all_gather(whole, 'sp', axis=0, tiled=True)  37.1 us
    all_gather x1, blocking collectives, on_device_by_column(): conv_all = lax.all_gather(conv_branch, 'sp')  32.3 us
    all_gather x1, blocking collectives, on_device_by_column(): lax.all_gather(jnp.concatenate([input_offset, forget_offset], axis=1), 's...  27.4 us
    all_to_all x1, blocking collectives, send_partials(): lax.all_to_all(partial.reshape(count, length // count, width), 'sp', 0, 0)  17.2 us
    all_to_all x1, blocking collectives, send_partials(): groups = lax.all_to_all(swapped, 'tp', 0, 0)  11.2 us
    all_gather x1, blocking collectives, gather_tokens(): whole = lax.all_gather(tokens, 'tp', axis=1, tiled=True)  10.4 us
  transfers between devices with their start and end apart: 4, of which 4 were waited for; matrix products, arithmetic and copies ran while one was open for 6% of the time, Pallas kernels for 0%

profile of v1, /device:TPU:0, one launch (start us, length us, event | category | flops | bytes accessed | tf_op | source)
XLA Modules:
  0.0 268.2 jit_solution(7176021752319690707)
XLA Ops:
  6.6 10.4 %all_gather.33 = bf16[128,2048]{1,0:T(8,128)(2,1)} all-gather(bf16[128,512]{1,0:T(8,128)(2,1)} %param.15), channel_id=1, replica_groups=mesh['sp'=8,'tp'=4] {'tp'}, dimensions={1}, use_global_device_ids=true | all-gather | bytes 655360 | tf_op jit(solution)/shard_map/all_gather | solution.py:219
  17.0 1.1 copy.40
  18.1 1.1 copy.41
  19.2 1.1 copy.42
  20.3 1.0 copy.43
  21.3 1.0 copy.44
  22.3 0.7 constant_dynamic-update-slice_fusion.4
  23.0 0.7 constant_dynamic-update-slice_fusion.3
  23.7 0.7 constant_dynamic-update-slice_fusion.2
  24.4 0.7 constant_dynamic-update-slice_fusion.1
  25.1 0.7 constant_dynamic-update-slice_fusion
  25.8 5.8 %all-to-all-start = ((bf16[8,256,256]{1,2,0:T(8,128)(2,1)}), bf16[8,256,256]{1,2,0:T(8,128)(2,1)S(1)}, u32[]{:S(2)}, u32[]{:S(2)}) async-start(bf16[8,256,256]{1,2,0:T(8,128)(2,1)} %bitcast.5), calls=%async_computation | async-start | bytes 2097152 | tf_op jit(solution)/shard_map/all_to_all | solution.py:215
  31.7 0.1 dynamic-slice_convert_fusion
  31.8 37.1 %all-to-all-done = bf16[8,256,256]{1,2,0:T(8,128)(2,1)S(1)} async-done(((bf16[8,256,256]{1,2,0:T(8,128)(2,1)}), bf16[8,256,256]{1,2,0:T(8,128)(2,1)S(1)}, u32[]{:S(2)}, u32[]{:S(2)}) %all-to-all-start) | async-done | bytes 1048608 | tf_op jit(solution)/shard_map/all_to_all | solution.py:215
  68.9 0.5 copy.45
  69.4 37.1 %all-gather.9.cloned.1.call-done = bf16[1024,2048]{1,0:T(8,128)(2,1)} async-done(((bf16[128,2048]{1,0:T(8,128)(2,1)}), bf16[1024,2048]{1,0:T(8,128)(2,1)}) %all-gather.9.cloned.1.call-update) | async-done | bytes 4194320 | tf_op jit(solution)/shard_map/all_gather | solution.py:220
  106.5 3.5 %convolution_bitcast_fusion.1 = f32[1024,256]{0,1:T(8,128)S(1)} fusion(bf16[2048,256]{1,0:T(8,128)(2,1)S(1)} %bitcast.145, bf16[1024,2048]{1,0:T(8,128)(2,1)} %all-gather.9.cloned.1.call-done), kind=kOutput, calls=%fused_computation.3 | convolution fusion | flops 1073741824 | bytes 6291456 | tf_op jit(solution)/shard_map/dot_general | solution.py:271
  110.0 0.8 slice.659
  110.9 0.1 dynamic_slice.36
  111.0 27.4 %all_gather.37 = f32[1024,4]{0,1:T(4,128)S(1)} all-gather(f32[128,4]{0,1:T(4,128)S(1)} %pad_maximum_fusion), channel_id=1, replica_groups=mesh['sp'=8,'tp'=4] {'sp'}, dimensions={0}, use_global_device_ids=true | all-gather | bytes 18432 | tf_op jit(solution)/shard_map/all_gather | solution.py:267
  138.5 3.4 %fusion.3 = f32[4,1024]{1,0:T(4,128)S(1)} fusion(f32[1024,4]{0,1:T(4,128)S(1)} %all_gather.37, bf16[1024,2048]{1,0:T(8,128)(2,1)} %all-gather.9.cloned.1.call-done, bf16[2048,2]{0,1:T(2,128)(2,1)S(1)} %copy-done.2, bf16[2048,2]{0,1:T(2,128)(2,1)S(1)} %copy-done.3), kind=kOutput, calls=%fused_computation.8 | convolution fusion | flops 16814080 | bytes 4243456 | tf_op jit(solution)/shard_map/dot_general | solution.py:272
  141.9 0.3 reduce-window.24
  142.3 0.3 reduce-window.16
  142.7 0.1 slice_reduce_fusion
  142.8 0.1 slice_reduce_fusion.1
  143.1 0.5 fusion.4
  143.6 1.3 fusion.81
  144.9 0.4 all-gather.11.cloned.1.call-done
  145.3 2.9 %reshape.162 = bf16[4,1024,192]{1,0,2:T(4,128)(2,1)S(1)} reshape(bf16[4096,192]{0,1:T(8,128)(2,1)} %all-gather.11.cloned.1.call-done) | data formatting | bytes 3145728 | tf_op jit(solution)/shard_map/all_gather | solution.py:226
  148.2 0.5 fusion.83
  148.8 0.7 fusion.85
  149.5 0.2 copy.56
  149.7 0.4 multiply_reduce_fusion
  150.1 41.8 %all-gather.4 = f32[32,3,1024]{2,1,0:T(4,128)S(1)} all-gather(f32[1,3,1024]{2,1,0:T(4,128)S(1)} %maximum_bitcast_fusion), channel_id=3, replica_groups=mesh['sp'=8,'tp'=4] {'sp','tp'}, dimensions={0}, use_global_device_ids=true | all-gather | bytes 405504 | tf_op jit(solution)/shard_map/all_gather | solution.py:311
  191.9 0.1 reduce_sum.61
  192.1 0.8 multiply_convert_fusion
  192.9 0.1 dynamic_slice.34
  193.0 0.1 multiply_convert_fusion.1
  193.1 32.3 %all-gather.2 = bf16[8192,32]{0,1:T(8,128)(2,1)S(1)} all-gather(bf16[1024,32]{0,1:T(8,128)(2,1)S(1)} %multiply_convert_fusion.1), channel_id=4, replica_groups=mesh['sp'=8,'tp'=4] {'sp'}, dimensions={0}, use_global_device_ids=true | all-gather | bytes 589824 | tf_op jit(solution)/shard_map/all_gather | solution.py:324
  225.4 4.7 %all-gather.13.cloned.1.call-done = bf16[2048,256]{0,1:T(8,128)(2,1)} async-done(((bf16[256,256]{0,1:T(8,128)(2,1)}), bf16[2048,256]{0,1:T(8,128)(2,1)}) %all-gather.13.cloned.1.call-update) | async-done | bytes 1048592 | tf_op jit(solution)/shard_map/all_gather | solution.py:325
  230.1 1.3 copy.69
  231.4 0.5 fusion.86
  231.9 0.4 fusion.1
  232.3 17.2 %all_to_all.15 = bf16[8,128,256]{2,1,0:T(8,128)(2,1)S(1)} all-to-all(bf16[8,128,256]{2,1,0:T(8,128)(2,1)S(1)} %bitcast.141), channel_id=1, replica_groups=mesh['sp'=8,'tp'=4] {'sp'}, dimensions={0} | all-to-all | bytes 1048576 | tf_op jit(solution)/shard_map/all_to_all | solution.py:340
  249.5 11.2 %all_to_all.16 = bf16[4,2,128,256]{3,2,1,0:T(8,128)(2,1)S(1)} all-to-all(bf16[4,2,128,256]{3,2,1,0:T(8,128)(2,1)S(1)} %bitcast.143), channel_id=1, replica_groups=mesh['sp'=8,'tp'=4] {'tp'}, dimensions={0} | all-to-all | bytes 1048576 | tf_op jit(solution)/shard_map/all_to_all | solution.py:342
  260.7 0.1 reduce_sum.62
  260.8 0.1 copy.51
  260.9 0.8 copy.52
  (49 shorter events, 0.9 us)
Async XLA Ops:
  6.5 224.9 %copy-start = (bf16[512,256]{1,0:T(8,128)(2,1)S(1)}, bf16[512,256]{1,0:T(8,128)(2,1)}, u32[]{:S(2)}) copy-start(bf16[512,256]{1,0:T(8,128)(2,1)} %param.29) | copy-start | bytes 786436
  6.5 25.1 %copy-start.5 = (f32[128,2]{0,1:T(2,128)S(1)}, f32[128,2]{0,1:T(2,128)}, u32[]{:S(2)}) copy-start(f32[128,2]{0,1:T(2,128)} %param.26) | copy-start | bytes 3076
  6.5 25.1 %copy-start.6 = (f32[128,2]{0,1:T(2,128)S(1)}, f32[128,2]{0,1:T(2,128)}, u32[]{:S(2)}) copy-start(f32[128,2]{0,1:T(2,128)} %param.25) | copy-start | bytes 3076
  6.5 25.1 %copy-start.4 = (bf16[31,256]{1,0:T(8,128)(2,1)S(1)}, bf16[31,256]{1,0:T(8,128)(2,1)}, u32[]{:S(2)}) copy-start(bf16[31,256]{1,0:T(8,128)(2,1)} %param.18) | copy-start | bytes 47620
  6.5 99.9 %all-gather.9.cloned.1.call-start = ((), (), s32[]{:S(2)}) async-start(), calls=%async_computation.3 | async-start | bytes 4718592 | tf_op jit(solution)/shard_map/all_gather | solution.py:220
  25.8 43.1 %all-to-all-start = ((bf16[8,256,256]{1,2,0:T(8,128)(2,1)}), bf16[8,256,256]{1,2,0:T(8,128)(2,1)S(1)}, u32[]{:S(2)}, u32[]{:S(2)}) async-start(bf16[8,256,256]{1,2,0:T(8,128)(2,1)} %bitcast.5), calls=%async_computation | async-start | bytes 2097152 | tf_op jit(solution)/shard_map/all_to_all | solution.py:215
  31.6 113.7 %all-gather.11.cloned.1.call-start = ((), (), s32[]{:S(2)}) async-start(), calls=%async_computation.4 | async-start | bytes 1966080 | tf_op jit(solution)/shard_map/all_gather | solution.py:226
  106.5 4.5 %copy-start.7 = (f32[512]{0:T(512)S(1)}, f32[512]{0:T(512)}, u32[]{:S(2)}) copy-start(f32[512]{0:T(512)} %param.27) | copy-start | bytes 6148
  106.5 32.0 %copy-start.2 = (bf16[2048,2]{0,1:T(2,128)(2,1)S(1)}, bf16[2048,2]{0,1:T(2,128)(2,1)}, u32[]{:S(2)}) copy-start(bf16[2048,2]{0,1:T(2,128)(2,1)} %param.24) | copy-start | bytes 24580
  106.5 32.0 %copy-start.3 = (bf16[2048,2]{0,1:T(2,128)(2,1)S(1)}, bf16[2048,2]{0,1:T(2,128)(2,1)}, u32[]{:S(2)}) copy-start(bf16[2048,2]{0,1:T(2,128)(2,1)} %param.23) | copy-start | bytes 24580
  110.8 119.3 %all-gather.13.cloned.1.call-start = ((), (), s32[]{:S(2)}) async-start(), calls=%async_computation.5 | async-start | bytes 1179648 | tf_op jit(solution)/shard_map/all_gather | solution.py:325
  148.8 44.1 %copy-start.8 = (f32[256]{0:T(256)S(1)}, f32[256]{0:T(256)}, u32[]{:S(2)}) copy-start(f32[256]{0:T(256)} %param.19) | copy-start | bytes 3076
  150.1 81.8 %copy-start.1 = (bf16[256,256]{1,0:T(8,128)(2,1)S(1)}, bf16[256,256]{1,0:T(8,128)(2,1)}, u32[]{:S(2)}) copy-start(bf16[256,256]{1,0:T(8,128)(2,1)} %param.28) | copy-start | bytes 393220
Sparse Core Ops, SparseCore 0:
  17.1 89.3 all-gather.8
  110.9 34.2 all-gather.10
  193.0 37.0 all-gather.12
